TPU v7x, 32 devices: a whole 2x2x4 slice. The times are simulated.
32 devices in a mesh: sp: 16 (over z, y, x), tp: 2 (over core).
Axes of the slice: x: 2, y: 2, z: 4, core: 2. Of those that a mesh axis runs over, the one named last changes fastest.
Arguments:
- prompt: bfloat16 [8, 1024, 2048], P(None, 'sp'), may hold values from -6 to 6
- keep_scale: float32 [8, 1024], P(None, 'sp'), may hold values from 0.25 to 1
- new_token: bfloat16 [8, 2048], P(None, 'tp'), may hold values from -6 to 6
- w_query: bfloat16 [2048, 1024], P(None, 'tp'), may hold values from -0.125 to 0.125
- w_forget: bfloat16 [2048, 1024], P(None, 'tp'), may hold values from -0.125 to 0.125
- w_value: bfloat16 [2048, 1024], P(None, 'tp'), may hold values from -2.109375 to 2.109375
- w_outgate: bfloat16 [2048, 1024], P(None, 'tp'), may hold values from -0.125 to 0.125
- floor_gap: float32 [1024], P('tp'), may hold values from 0 to 0.06
- norm_gain: float32 [128], replicated, may hold values from 0.1 to 1.9
Outputs:
- state_cache: bfloat16 [8, 1024, 128], P('tp', 'sp')
- first_read: bfloat16 [8, 1024], P(None, 'tp')
All inputs are finite; a program needn't handle non-finite values.
Results may differ from a plain program's by a relative error of at most 0.0022.
The roundings to bfloat16 on the way count: a program that leaves them out, or rounds other values in their place, can miss the bound.
Values may be sent and summed in bfloat16 or wider, within the bound.
A program may use at most 64 MiB of HBM per device.

v0:
```python
import jax
import jax.numpy as jnp
from jax import lax
from jax.sharding import PartitionSpec as P

HIGHEST_PRECISION = lax.Precision.HIGHEST
EPSILON = 1e-06


def entering(value, axis, join, neutral):
    count, mine = (lax.axis_size(axis), lax.axis_index(axis))
    pieces = lax.all_gather(value, axis)
    pieces = pieces[::-1]
    mine = count - 1 - mine
    total = jnp.full_like(value, 0) + jnp.asarray(neutral, value.dtype)

    def hop(position, total):
        longer = join(total, pieces[position])
        return jnp.where(position < mine, longer, total)

    return lax.fori_loop(0, count - 1, hop, total)


def add_totals(earlier, following):
    return earlier + following


def later_totals(block_log):
    return entering(block_log, "sp", add_totals, jnp.zeros_like(block_log))


def per_device(
    prompt, keep_scale, new_token, w_query, w_forget, w_value, w_outgate, floor_gap, norm_gain
):
    sequences, positions, model_width = prompt.shape
    head_size = norm_gain.shape[0]
    local_heads = w_forget.shape[1] // head_size
    flattened = prompt.reshape(sequences * positions, model_width)
    forget_pre = jnp.dot(flattened, w_forget, preferred_element_type=jnp.float32)
    forget_pre = forget_pre.reshape(sequences, positions, local_heads, head_size)
    values = jnp.dot(flattened, w_value, preferred_element_type=jnp.float32).astype(jnp.bfloat16)
    values = lax.optimization_barrier(values).astype(jnp.float32)
    values = values.reshape(sequences, positions, local_heads, head_size)
    floor_rows = floor_gap.reshape(local_heads, head_size)
    forget_loss = floor_rows * (1.0 - jax.nn.sigmoid(forget_pre))
    keep_factor = keep_scale[:, :, None, None]
    log_forget = jnp.log(keep_factor) + jnp.log1p(-forget_loss)
    input_gate = 1.0 - keep_factor + keep_factor * forget_loss
    inside_log = lax.cumsum(log_forget, axis=1, reverse=True) - log_forget
    block_log = jnp.sum(log_forget, axis=1).transpose(1, 0, 2)
    states = jnp.einsum(
        "sthc,sthv->hscv", input_gate * jnp.exp(inside_log), values, precision=HIGHEST_PRECISION
    )
    later_log = None
    later_log = later_totals(block_log)
    decayed = states * jnp.exp(later_log)[..., None]
    final_rows = lax.psum_scatter(
        decayed.reshape(local_heads, sequences * head_size, head_size),
        "sp",
        scatter_dimension=1,
        tiled=True,
    )
    weights = (w_query, w_forget, w_value, w_outgate)
    portion = lax.all_gather(new_token, "tp", axis=1, tiled=True)
    query, new_forget, new_value, new_gate = tuple(
        (jnp.dot(portion, weight, preferred_element_type=jnp.float32) for weight in weights)
    )
    shaped = (sequences, local_heads, head_size)
    new_value = (
        lax.optimization_barrier(new_value.astype(jnp.bfloat16)).astype(jnp.float32).reshape(shaped)
    )
    query = query.reshape(shaped)
    new_forget = new_forget.reshape(shaped)
    new_gate = new_gate.reshape(shaped)
    new_loss = floor_rows * (1.0 - jax.nn.sigmoid(new_forget))
    read_weight = (query * (1.0 - new_loss)).transpose(1, 0, 2)
    read_part = jnp.einsum(
        "hsc,hscv->hsv", read_weight * jnp.exp(later_log), states, precision=HIGHEST_PRECISION
    )
    mixed_read = lax.psum(read_part, "sp").transpose(1, 0, 2)
    own_term = jnp.sum(query * new_loss, axis=-1, keepdims=True)
    mixed_read = mixed_read + own_term * new_value
    normed = mixed_read * lax.rsqrt(
        jnp.mean(mixed_read * mixed_read, axis=-1, keepdims=True) + EPSILON
    )
    first_read = (normed * norm_gain * jax.nn.silu(new_gate)).reshape(
        sequences, local_heads * head_size
    )
    return (final_rows.astype(jnp.bfloat16), first_read.astype(jnp.bfloat16))


def solution(mesh):
    return jax.shard_map(
        per_device,
        mesh=mesh,
        in_specs=(
            P(None, "sp", None),
            P(None, "sp"),
            P(None, "tp"),
            P(None, "tp"),
            P(None, "tp"),
            P(None, "tp"),
            P(None, "tp"),
            P("tp"),
            P(),
        ),
        out_specs=(P("tp", "sp", None), P(None, "tp")),
        check_vma=False,
    )
```

profile of v0, /device:TPU:0, one launch (start us, length us, event | category | flops | bytes accessed | tf_op | source)
XLA Modules:
  0.0 164.8 jit_solution(11791503214034066213)
XLA Ops:
  7.2 0.0 copy-start
  7.2 0.0 reduce-scatter.2.cloned.1.call-start
  7.2 0.8 broadcast_subtract_fusion
  8.1 4.0 %copy.26 = bf16[512,2048]{1,0:T(8,128)(2,1)} copy(bf16[512,2048]{0,1:T(8,128)(2,1)} %bitcast.70) | data formatting | bytes 4194304 | tf_op jit(solution)/shard_map/dot_general | solution.py:39
  12.0 0.0 copy-done
  12.0 0.0 copy-done.7
  12.1 4.7 %fusion.38 = (f32[8,4,128]{2,1,0:T(4,128)S(1)}, f32[8,64,4,128]{3,1,2,0:T(8,128)}, f32[8,64,4,128]{3,1,2,0:T(8,128)}) fusion(f32[8,64]{1,0:T(8,128)S(1)} %get-tuple-element.110, bf16[4,128,2048,1]{2,1,0,3:T(8,128)(2,1)} %bitcast.72, bf16[8,64,2048]{2,1,0:T(8,128)(2,1)S(1)} %copy-done, f32[4,128]{1,0:T(4,128)S(1)} %bitcast.76), kind=kOutput, calls=%fused_computation.35 | convolution fusion | flops 1075834880 | bytes 6311936 | tf_op jit(solution)/shard_map/dot_general | solution.py:39
  16.8 43.8 %all-gather = f32[64,8,128]{2,1,0:T(8,128)S(1)} all-gather(f32[4,8,128]{2,1,0:T(8,128)S(1)} %copy.21), channel_id=2, replica_groups=mesh['sp'=16,'tp'=2] {'sp'}, dimensions={0}, use_global_device_ids=true | all-gather | bytes 278528 | tf_op jit(solution)/shard_map/all_gather | solution.py:12
  60.6 0.6 while.14
  61.2 0.0 copy-done.6
  61.2 0.0 copy-start.1
  61.2 2.0 %all_gather.11 = bf16[8,2048]{1,0:T(8,128)(2,1)S(1)} all-gather(bf16[8,1024]{1,0:T(8,128)(2,1)S(1)} %copy-done.6), channel_id=1, replica_groups=mesh['sp'=16,'tp'=2] {'tp'}, dimensions={1}, use_global_device_ids=true | all-gather | bytes 49152 | tf_op jit(solution)/shard_map/all_gather | solution.py:64
  63.2 2.1 %fusion.30 = f32[8,4,128]{2,0,1:T(8,128)S(1)} fusion(bf16[8,2048]{1,0:T(8,128)(2,1)S(1)} %all_gather.11, bf16[2048,512]{1,0:T(8,128)(2,1)} %param.15, f32[4,128]{1,0:T(4,128)S(1)} %bitcast.77), kind=kOutput, calls=%fused_computation.22 | convolution fusion | flops 16797696 | bytes 2148352 | tf_op jit(solution)/shard_map/dot_general | solution.py:66
  65.2 0.0 copy-done.1
  65.2 0.0 copy-start.2
  65.3 0.4 convolution_bitcast_fusion.1
  65.6 0.0 copy-done.4
  65.6 1.4 fusion.35
  67.1 0.0 copy-start.5
  67.1 2.1 %convolution_convert_fusion = bf16[512,512]{1,0:T(8,128)(2,1)} fusion(bf16[512,2048]{1,0:T(8,128)(2,1)S(1)} %bitcast.69, bf16[2048,512]{1,0:T(8,128)(2,1)S(1)} %copy-done.2), kind=kOutput, calls=%fused_computation.12 | convolution fusion | flops 1074003968 | bytes 4718592 | tf_op jit(solution)/shard_map/dot_general | solution.py:41
  69.2 2.0 %reshape.57 = bf16[8,64,4,128]{3,2,1,0:T(4,128)(2,1)} reshape(bf16[512,512]{1,0:T(8,128)(2,1)} %convolution_convert_fusion) | data formatting | bytes 1048576 | tf_op jit(solution)/shard_map/reshape | solution.py:43
  71.1 0.0 copy-done.5
  71.1 6.0 %broadcast_multiply_fusion = (f32[4,8,128,128]{3,2,1,0:T(8,128)}, f32[4,8,128,128]{3,2,1,0:T(8,128)}) fusion(f32[4,8,128]{2,1,0:T(8,128)S(1)} %get-tuple-element.108, bf16[8,64,4,128]{3,2,1,0:T(4,128)(2,1)} %reshape.57, f32[8,64,4,128]{3,0,1,2:T(8,128)S(1)} %fusion.35, f32[8,64,4,128]{3,1,2,0:T(8,128)} %get-tuple-element.111, f32[8,64]{1,0:T(8,128)S(1)} %copy-done.5, ...), kind=kOutput, calls=%fused_computation.32 | convolution fusion | flops 404750336 | bytes 6838272 | tf_op jit(solution)/shard_map/sthc,sthv->hscv/dot_general | solution.py:51
  77.1 0.0 reduce-scatter.2.cloned.1.call-update
  77.2 0.0 copy-start.3
  77.2 0.0 copy-start.8
  77.2 3.6 %fusion.3 = f32[8,4,1,128]{3,2,1,0:T(1,128)S(1)} fusion(f32[4,8,128,128]{3,2,1,0:T(8,128)} %get-tuple-element.113, f32[4,8,128,1]{2,1,0,3:T(8,128)S(1)} %get-tuple-element.107), kind=kOutput, calls=%fused_computation.4 | convolution fusion | flops 6291456 | bytes 2129920 | tf_op jit(solution)/shard_map/hsc,hscv->hsv/dot_general | solution.py:77
  80.8 0.4 convolution_convert_fusion.1
  81.2 72.0 %psum.7 = f32[8,4,128]{2,0,1:T(8,128)S(1)} all-reduce(f32[8,4,128]{2,0,1:T(8,128)S(1)} %bitcast.74), channel_id=1, replica_groups=mesh['sp'=16,'tp'=2] {'sp'}, use_global_device_ids=true, to_apply=%region_5.6 | all-reduce | flops 4096 | bytes 32768 | tf_op jit(solution)/shard_map/psum | solution.py:80
  153.1 0.6 multiply_reduce_fusion
  153.8 2.6 %fusion.41 = bf16[8,512]{1,0:T(8,128)(2,1)} fusion(bf16[8,2048]{1,0:T(8,128)(2,1)S(1)} %all_gather.11, bf16[2048,512]{1,0:T(8,128)(2,1)} %param.17, f32[8,4,128]{2,0,1:T(8,128)S(1)} %get-tuple-element.115, f32[128]{0:T(128)S(1)} %copy-done.8, f32[8,4]{0,1:T(4,128)S(1)} %add_rsqrt_fusion), kind=kOutput, calls=%fused_computation.41 | convolution fusion | flops 16809984 | bytes 2155136 | tf_op jit(solution)/shard_map/dot_general | solution.py:66
  156.4 1.5 convert_element_type.18
  (28 shorter events, 0.2 us)
Async XLA Ops:
  7.2 4.9 %copy-start = (bf16[8,64,2048]{2,1,0:T(8,128)(2,1)S(1)}, bf16[8,64,2048]{2,1,0:T(8,128)(2,1)}, u32[]{:S(2)}) copy-start(bf16[8,64,2048]{2,1,0:T(8,128)(2,1)} %param.11) | copy-start | bytes 6291460
  7.2 149.2 %reduce-scatter.2.cloned.1.call-start = ((), (), s32[]{:S(2)}) async-start(), calls=%async_computation.1 | async-start | bytes 2228224 | tf_op jit(solution)/shard_map/reduce_scatter | solution.py:57
  8.1 4.0 %copy-start.7 = (f32[512]{0:T(512)S(1)}, f32[512]{0:T(512)}, u32[]{:S(2)}) copy-start(f32[512]{0:T(512)} %param.18) | copy-start | bytes 6148
  12.1 49.1 %copy-start.6 = (bf16[8,1024]{1,0:T(8,128)(2,1)S(1)}, bf16[8,1024]{1,0:T(8,128)(2,1)}, u32[]{:S(2)}) copy-start(bf16[8,1024]{1,0:T(8,128)(2,1)} %param.13) | copy-start | bytes 49156
  61.2 4.1 %copy-start.1 = (bf16[2048,512]{1,0:T(8,128)(2,1)S(1)}, bf16[2048,512]{1,0:T(8,128)(2,1)}, u32[]{:S(2)}) copy-start(bf16[2048,512]{1,0:T(8,128)(2,1)} %param.14) | copy-start | bytes 6291460
  63.2 2.5 %copy-start.4 = (f32[8,64,4,128]{3,1,2,0:T(8,128)S(1)}, f32[8,64,4,128]{3,1,2,0:T(8,128)}, u32[]{:S(2)}) copy-start(f32[8,64,4,128]{3,1,2,0:T(8,128)} %get-tuple-element.106) | copy-start | bytes 3145732
  65.2 1.8 %copy-start.2 = (bf16[2048,512]{1,0:T(8,128)(2,1)S(1)}, bf16[2048,512]{1,0:T(8,128)(2,1)}, u32[]{:S(2)}) copy-start(bf16[2048,512]{1,0:T(8,128)(2,1)} %param.16) | copy-start | bytes 6291460
  67.1 4.1 %copy-start.5 = (f32[8,64]{1,0:T(8,128)S(1)}, f32[8,64]{1,0:T(8,128)}, u32[]{:S(2)}) copy-start(f32[8,64]{1,0:T(8,128)} %param.12) | copy-start | bytes 6148
  77.2 3.6 %copy-start.3 = (bf16[2048,512]{1,0:T(8,128)(2,1)S(1)}, bf16[2048,512]{1,0:T(8,128)(2,1)}, u32[]{:S(2)}) copy-start(bf16[2048,512]{1,0:T(8,128)(2,1)} %param.16) | copy-start | bytes 6291460
  77.2 76.6 %copy-start.8 = (f32[128]{0:T(128)S(1)}, f32[128]{0:T(128)}, u32[]{:S(2)}) copy-start(f32[128]{0:T(128)} %param.19) | copy-start | bytes 1540
Sparse Core Ops, SparseCore 0:
  77.3 77.4 reduce-scatter.1
where the time goes:
time: 165 us
  blocking collectives  118 us (72%)
  matrix products  21.8 us (13%)
  between operations  14.2 us (9%)
  local copies, waits for them, and re-layouts  6.02 us (4%)
  other arithmetic  4.62 us (3%)
    psum x1, blocking collectives, per_device(): mixed_read = lax.psum(read_part, 'sp').transpose(1, 0, 2)  72 us
    all_gather x1, blocking collectives, entering(): pieces = lax.all_gather(value, axis)  43.8 us
    dot_general x1, matrix products, per_device(): jnp.einsum('sthc,sthv->hscv', input_gate * jnp.exp(inside_log), values, p...  5.99 us
    dot_general x4, matrix products, per_device(): jnp.dot(portion, weight, preferred_element_type=jnp.float32)  5.44 us
    dot_general x1, matrix products, per_device(): jnp.dot(flattened, w_forget, preferred_element_type=jnp.float32)  4.71 us
    dot_general x1, local copies, waits for them, and re-layouts, per_device(): jnp.dot(flattened, w_forget, preferred_element_type=jnp.float32)  3.97 us
    dot_general x1, matrix products, per_device(): jnp.einsum('hsc,hscv->hsv', read_weight * jnp.exp(later_log), states, pre...  3.6 us
  transfers between devices with their start and end apart: 1, of which 0 were waited for; matrix products, arithmetic and copies ran while one was open for 4% of the time, Pallas kernels for 0%

commit v1 on v0

v1 whole, which is shorter than its diff:
```python
import functools

import jax
import jax.numpy as jnp
from jax import lax
from jax.experimental import pallas as pl
from jax.experimental.pallas import tpu as pltpu
from jax.sharding import PartitionSpec as P

EPSILON = 1e-06
MESH = pl.DeviceIdType.MESH
F32 = jnp.float32
BF16 = jnp.bfloat16


def swap(mine, step, count):
    if count & (count - 1):
        return lax.rem(step - mine + 2 * count, count)
    total, bit = 0, 1
    while bit < count:
        total = total + bit * lax.rem(lax.rem(mine // bit, 2) + lax.rem(step // bit, 2), 2)
        bit *= 2
    return total


def pieces(x, count):
    out = []
    for _ in range(count):
        piece = x.astype(BF16)
        out.append(piece)
        x = x - piece.astype(F32)
    return out


def kernel(
    sizes,
    prompt, keep, token, w_query, w_forget, w_value, w_outgate, floor, gain,
    cache_out, read_out,
    blocks, keeps, tokens, wq, wf, wv, wo, weighted, values, logs, states, got_states, reads, sums,
    local_sem, direct_send, direct_recv, keep_send, keep_recv, fwd_send, fwd_recv,
    token_send, token_recv, log_send, log_recv, state_send, state_recv, read_send, read_recv,
):
    n, t, s_count, group, heads, head, rows = sizes
    me, core = lax.axis_index("sp"), lax.axis_index("tp")
    mine, place = me // group, lax.rem(me, group)
    model = prompt.shape[2]
    part = model // t
    positions = prompt.shape[1]
    width = heads * head

    def columns(c):
        return pl.ds(pl.multiple_of(c * part, part), part)

    def order(i):
        half = s_count // 2
        if s_count % 2:
            return i
        return 2 * lax.rem(half - i // 2, half) + lax.rem(i, 2)

    def peer(i):
        return swap(mine, order(i), s_count)

    local = [
        pltpu.make_async_copy(prompt.at[mine], blocks.at[mine], local_sem.at[0]),
        pltpu.make_async_copy(w_forget, wf, local_sem.at[1]),
        pltpu.make_async_copy(w_value, wv, local_sem.at[2]),
        pltpu.make_async_copy(w_query, wq, local_sem.at[3]),
        pltpu.make_async_copy(w_outgate, wo, local_sem.at[4]),
    ]

    barrier = pltpu.get_barrier_semaphore()
    for o in range(1, n):
        pl.semaphore_signal(barrier, inc=1, device_id=(lax.rem(me + o, n), core), device_id_type=MESH)
    for o in range(1, t):
        pl.semaphore_signal(barrier, inc=1, device_id=(me, lax.rem(core + o, t)), device_id_type=MESH)
    for copy in local:
        copy.start()
    pl.semaphore_wait(barrier, n - 1 + t - 1)

    def direct(i):
        to = peer(i)
        return pltpu.make_async_remote_copy(
            src_ref=prompt.at[to, :, columns(core)],
            dst_ref=blocks.at[mine, :, columns(core)],
            send_sem=direct_send.at[i], recv_sem=direct_recv.at[i],
            device_id=(to * group + place, core), device_id_type=MESH,
        )

    def direct_in(i):
        frm = peer(i)
        return pltpu.make_async_remote_copy(
            src_ref=prompt.at[frm, :, columns(core)],
            dst_ref=blocks.at[frm, :, columns(core)],
            send_sem=direct_send.at[i], recv_sem=direct_recv.at[i],
            device_id=(frm * group + place, core), device_id_type=MESH,
        )

    def keep_copy(i):
        to = peer(i)
        return pltpu.make_async_remote_copy(
            src_ref=keep, dst_ref=keeps.at[i],
            send_sem=keep_send.at[i], recv_sem=keep_recv.at[i],
            device_id=(to * group + place, core), device_id_type=MESH,
        )

    def forward(i, o):
        frm = peer(i)
        return pltpu.make_async_remote_copy(
            src_ref=blocks.at[frm, :, columns(core)],
            dst_ref=blocks.at[frm, :, columns(core)],
            send_sem=fwd_send.at[i, o], recv_sem=fwd_recv.at[i, o],
            device_id=(me, lax.rem(core + o, t)), device_id_type=MESH,
        )

    def forward_in(i, o):
        frm = peer(i)
        c = lax.rem(core - o + t, t)
        return pltpu.make_async_remote_copy(
            src_ref=blocks.at[frm, :, columns(c)],
            dst_ref=blocks.at[frm, :, columns(c)],
            send_sem=fwd_send.at[i, o], recv_sem=fwd_recv.at[i, o],
            device_id=(me, lax.rem(core + o, t)), device_id_type=MESH,
        )

    def token_copy(o, c):
        return pltpu.make_async_remote_copy(
            src_ref=token, dst_ref=tokens.at[c],
            send_sem=token_send.at[o], recv_sem=token_recv.at[o],
            device_id=(me, lax.rem(core + o, t)), device_id_type=MESH,
        )

    for i in range(1, s_count):
        keep_copy(i).start()
        direct(i).start()
    for o in range(1, t):
        token_copy(o, core).start()

    keeps[0] = keep[...]
    tokens[core] = token[...]
    floor_row = floor[...]

    def forget(j, i):
        pre = jnp.dot(blocks[j], wf[...], preferred_element_type=F32)
        loss = floor_row * (1.0 / (1.0 + jnp.exp(pre)))
        row = keeps[i, pl.ds(mine, 1), :]
        r = lax.broadcasted_iota(jnp.int32, (positions, positions), 0)
        c = lax.broadcasted_iota(jnp.int32, (positions, positions), 1)
        scale = jnp.sum(jnp.where(r == c, jnp.broadcast_to(row, (positions, positions)), 0.0), axis=1, keepdims=True)
        log_forget = jnp.log(scale) + jnp.log1p(-loss)
        gate = 1.0 - scale + scale * loss
        later = jnp.where(c > r, 1.0, 0.0).astype(BF16)
        inside = sum(jnp.dot(later, p, preferred_element_type=F32) for p in pieces(log_forget, 3))
        logs[0, pl.ds(j, 1), :] = inside[0:1] + log_forget[0:1]
        weighted[j] = gate * jnp.exp(inside)

    def value(j):
        values[j] = jnp.dot(blocks[j], wv[...], preferred_element_type=F32).astype(BF16)

    local[0].wait()
    local[1].wait()
    local[2].wait()
    forget(mine, 0)
    value(mine)

    local[3].wait()
    local[4].wait()
    for o in range(1, t):
        token_copy(o, lax.rem(core - o + t, t)).wait_recv()
    feature = jnp.concatenate([tokens[c] for c in range(t)], axis=1)
    query = jnp.dot(feature, wq[...], preferred_element_type=F32)
    new_forget = jnp.dot(feature, wf[...], preferred_element_type=F32)
    new_value = jnp.dot(feature, wv[...], preferred_element_type=F32).astype(BF16).astype(F32)
    new_gate = jnp.dot(feature, wo[...], preferred_element_type=F32)
    new_loss = floor_row * (1.0 / (1.0 + jnp.exp(new_forget)))
    read_weight = query * (1.0 - new_loss)
    own = query * new_loss
    silu = new_gate * (1.0 / (1.0 + jnp.exp(-new_gate)))
    sums[0] = own
    sums[1] = new_value
    sums[2] = silu
    seq = lax.broadcasted_iota(jnp.int32, read_weight.shape, 0)
    sums[3] = jnp.broadcast_to(
        jnp.sum(jnp.where(seq == mine, read_weight, 0.0), axis=0, keepdims=True), read_weight.shape
    )

    def arrive(i):
        direct_in(i).wait_recv()
        for o in range(1, t):
            forward(i, o).start()

    def ready(i):
        keep_copy(i).wait_recv()
        for o in range(1, t):
            forward_in(i, o).wait_recv()

    arrive(1)

    def step(i, carry):
        arrive(i)
        ready(i - 1)
        j = peer(i - 1)
        forget(j, i - 1)
        value(j)
        return carry

    lax.fori_loop(2, s_count, step, 0)
    last = s_count - 1
    ready(last)
    j = peer(last)
    forget(j, last)

    def log_copy(o):
        return pltpu.make_async_remote_copy(
            src_ref=logs.at[0], dst_ref=logs.at[o],
            send_sem=log_send.at[o], recv_sem=log_recv.at[o],
            device_id=(mine * group + lax.rem(place + o, group), core), device_id_type=MESH,
        )

    for o in range(1, group):
        log_copy(o).start()
    value(j)
    for o in range(1, group):
        log_copy(o).wait_recv()

    own_log = logs[0]
    total, beside = own_log, jnp.zeros_like(own_log)
    for o in range(1, group):
        other = logs[o]
        total = total + other
        beside = beside + jnp.where(lax.rem(place - o + group, group) > place, other, 0.0)
    suffix = jnp.zeros((1, width), F32)
    for b in reversed(range(s_count)):
        weighted[b] = weighted[b] * jnp.exp(suffix + beside[b : b + 1])
        suffix = suffix + total[b : b + 1]

    def state_copy(o):
        to = lax.rem(place + o, group)
        return pltpu.make_async_remote_copy(
            src_ref=states.at[:, pl.ds(pl.multiple_of(to * rows, rows), rows), :], dst_ref=got_states.at[o],
            send_sem=state_send.at[o], recv_sem=state_recv.at[o],
            device_id=(mine * group + to, core), device_id_type=MESH,
        )

    def read_copy(o, sender):
        return pltpu.make_async_remote_copy(
            src_ref=reads.at[sender], dst_ref=reads.at[sender],
            send_sem=read_send.at[o], recv_sem=read_recv.at[o],
            device_id=(lax.rem(me + o, n), core), device_id_type=MESH,
        )

    for h in range(heads):
        lanes = slice(h * head, (h + 1) * head)
        w = weighted[:, :, lanes].reshape(s_count * positions, head)
        v = values[:, :, lanes].reshape(s_count * positions, head)
        state = sum(
            lax.dot_general(p, v, (((0,), (0,)), ((), ())), preferred_element_type=F32) for p in pieces(w, 2)
        )
        states[h] = state
        part_read = jnp.dot(sums[3, :, lanes], state, preferred_element_type=F32, precision=lax.Precision.HIGHEST)
        reads[me, :, lanes] = part_read[0:1]

    for o in range(n - 1, 0, -1):
        read_copy(o, me).start()
    for o in range(1, group):
        state_copy(o).start()

    start = pl.multiple_of(place * rows, rows)
    for o in range(1, group):
        state_copy(o).wait_recv()
    final = states[:, pl.ds(start, rows), :]
    for o in range(1, group):
        final = final + got_states[o]
    cache_out[...] = final.astype(BF16)

    for o in range(1, n):
        read_copy(o, lax.rem(me - o + n, n)).wait_recv()
    for s in range(s_count):
        row = reads[s * group]
        for g in range(1, group):
            row = row + reads[s * group + g]
        sums[4, s : s + 1, :] = row
    for h in range(heads):
        lanes = slice(h * head, (h + 1) * head)
        mixed = sums[4, :, lanes] + jnp.sum(sums[0, :, lanes], axis=1, keepdims=True) * sums[1, :, lanes]
        normed = mixed * lax.rsqrt(jnp.mean(mixed * mixed, axis=1, keepdims=True) + EPSILON)
        read_out[:, lanes] = (normed * gain[...] * sums[2, :, lanes]).astype(BF16)

    for i in range(1, s_count):
        keep_copy(i).wait_send()
        direct(i).wait_send()
        for o in range(1, t):
            forward(i, o).wait_send()
    for o in range(1, t):
        token_copy(o, core).wait_send()
    for o in range(1, group):
        log_copy(o).wait_send()
        state_copy(o).wait_send()
    for o in range(1, n):
        read_copy(o, me).wait_send()


def per_device(prompt, keep_scale, new_token, w_query, w_forget, w_value, w_outgate, floor_gap, norm_gain):
    n, t = lax.axis_size("sp"), lax.axis_size("tp")
    s_count, positions, model = prompt.shape
    head = norm_gain.shape[0]
    width = w_forget.shape[1]
    heads = width // head
    group = n // s_count
    rows = head // group
    sizes = (n, t, s_count, group, heads, head, rows)
    dma = pltpu.SemaphoreType.DMA
    vmem = pl.BlockSpec(memory_space=pltpu.VMEM)
    hbm = pl.BlockSpec(memory_space=pl.ANY)
    return pl.pallas_call(
        functools.partial(kernel, sizes),
        out_shape=(
            jax.ShapeDtypeStruct((heads, rows, head), BF16),
            jax.ShapeDtypeStruct((s_count, width), BF16),
        ),
        in_specs=[hbm, vmem, vmem, hbm, hbm, hbm, hbm, vmem, vmem],
        out_specs=(vmem, vmem),
        scratch_shapes=[
            pltpu.VMEM((s_count, positions, model), BF16),
            pltpu.VMEM((s_count,) + keep_scale.shape, F32),
            pltpu.VMEM((t,) + new_token.shape, BF16),
            pltpu.VMEM((model, width), BF16),
            pltpu.VMEM((model, width), BF16),
            pltpu.VMEM((model, width), BF16),
            pltpu.VMEM((model, width), BF16),
            pltpu.VMEM((s_count, positions, width), F32),
            pltpu.VMEM((s_count, positions, width), BF16),
            pltpu.VMEM((group, s_count, width), F32),
            pltpu.VMEM((heads, head, head), F32),
            pltpu.VMEM((group, heads, rows, head), F32),
            pltpu.VMEM((n, 1, width), F32),
            pltpu.VMEM((5, s_count, width), F32),
            dma((5,)),
            dma((s_count,)), dma((s_count,)),
            dma((s_count,)), dma((s_count,)),
            dma((s_count, t)), dma((s_count, t)),
            dma((t,)), dma((t,)),
            dma((group,)), dma((group,)),
            dma((group,)), dma((group,)),
            dma((n,)), dma((n,)),
        ],
        compiler_params=pltpu.CompilerParams(collective_id=0, has_side_effects=True),
    )(
        prompt, keep_scale, new_token, w_query, w_forget, w_value, w_outgate,
        floor_gap.reshape(1, width), norm_gain.reshape(1, head),
    )


def solution(mesh):
    return jax.shard_map(
        per_device,
        mesh=mesh,
        in_specs=(
            P(None, "sp", None),
            P(None, "sp"),
            P(None, "tp"),
            P(None, "tp"),
            P(None, "tp"),
            P(None, "tp"),
            P(None, "tp"),
            P("tp"),
            P(),
        ),
        out_specs=(P("tp", "sp", None), P(None, "tp")),
        check_vma=False,
    )
```

time: 165 us -> 51.8 us (0.31)
  blocking collectives: 118 us -> 0 us
  Pallas kernels: 0 us -> 48.1 us
  matrix products: 21.8 us -> 0 us
  between operations: 14.2 us -> 0.64 us
  other arithmetic: 4.62 us -> 0 us
  local copies, waits for them, and re-layouts: 6.02 us -> 2.77 us
    psum x1 -> x0, blocking collectives: 72 us -> none  [per_device(): mixed_read = lax.psum(read_part, 'sp').transpose(1, 0, 2)]
    pallas_call x0 -> x1, Pallas kernels: none -> 48.1 us  [per_device(): pl.pallas_call(functools.partial(kernel, sizes), out_shape=(jax.ShapeDtyp...]
    all_gather x2 -> x0, blocking collectives: 45.7 us -> none  [the longest x1 43.8 us: entering(): pieces = lax.all_gather(value, axis)]
    dot_general x8 -> x0, matrix products: 21.8 us -> none  [the longest x1 5.99 us: per_device(): jnp.einsum('sthc,sthv->hscv', input_gate * jnp.exp(inside_log), values, p...]
    dot_general x2 -> x0, local copies, waits for them, and re-layouts: 3.98 us -> none  [the longest x1 3.97 us: per_device(): jnp.dot(flattened, w_forget, preferred_element_type=jnp.float32)]
    unnamed x18 -> x2, local copies, waits for them, and re-layouts: 0.05 us -> 2.77 us
    reshape x1 -> x0, local copies, waits for them, and re-layouts: 1.97 us -> none  [per_device(): values = values.reshape(sequences, positions, local_heads, head_size)]
  transfers between devices with their start and end apart: 1 -> 0, of which waited for: 0 -> 0; matrix products, arithmetic and copies ran while one was open for 4% -> 0% of each run, Pallas kernels for 0% -> 0%
where the time goes in v1:
time: 51.8 us; the launch traced here: 51.5 us
  Pallas kernels  48.1 us (93%)
  local copies, waits for them, and re-layouts  2.77 us (5%)
  between operations  0.64 us (1%)
    pallas_call x1, Pallas kernels, per_device(): pl.pallas_call(functools.partial(kernel, sizes), out_shape=(jax.ShapeDtyp...  48.1 us
    unnamed x2, local copies, waits for them, and re-layouts  2.77 us

profile of v1, /device:TPU:0, one launch (start us, length us, event | category | flops | bytes accessed | tf_op | source)
XLA Modules:
  0.0 51.5 jit_solution(3951955410785686875)
XLA Ops:
  0.6 48.1 %shard_map.104 = (bf16[4,64,128]{2,1,0:T(8,128)(2,1)}, bf16[8,512]{1,0:T(8,128)(2,1)}) custom-call(bf16[8,64,2048]{2,1,0:T(8,128)(2,1)} %prompt.1, f32[8,64]{1,0:T(8,128)} %keep.1, bf16[8,1024]{1,0:T(8,128)(2,1)} %token_.1, bf16[2048,512]{1,0:T(8,128)(2,1)} %w_query.1, bf16[2048,512]{1,0:T(8,128)(2,1)} %w_forget.1, bf16[2048,512]{1,0:T(8,128)(2,1)} %w_value.1, ...), custom_call_target="tpu_custom_call" | custom-call | tf_op jit(solution)/shard_map/pallas_call | solution.py:314
  48.7 1.5 %copy.13 = bf16[4,64,128]{2,1,0:T(8,128)(2,1)} copy(bf16[4,64,128]{2,1,0:T(8,128)(2,1)} %get-tuple-element.4) | data formatting | bytes 131072
  50.2 1.3 %copy.14 = bf16[8,512]{1,0:T(8,128)(2,1)} copy(bf16[8,512]{1,0:T(8,128)(2,1)} %get-tuple-element.5) | data formatting | bytes 16384

commit v2 on v1

v2 whole, which is shorter than its diff:
```python
import functools

import jax
import jax.numpy as jnp
from jax import lax
from jax.experimental import pallas as pl
from jax.experimental.pallas import tpu as pltpu
from jax.sharding import PartitionSpec as P

EPSILON = 1e-06
MESH = pl.DeviceIdType.MESH
F32 = jnp.float32
BF16 = jnp.bfloat16


def partner(mine, step, count):
    total, bit = 0, 1
    while bit < count:
        total = total + bit * lax.rem(lax.rem(mine // bit, 2) + lax.rem(step // bit, 2), 2)
        bit *= 2
    return total


def pieces(x, count):
    out = []
    for _ in range(count):
        piece = x.astype(BF16)
        out.append(piece)
        x = x - piece.astype(F32)
    return out


def kernel(
    sizes,
    prompt, keep, token, w_query, w_forget, w_value, w_outgate, floor, gain,
    cache_out, read_out,
    blocks, keeps, tokens, wq, wf, wv, wo, weighted, values, logs, totals, got_totals, states, got_states, reads, sums,
    local_sem, direct_send, direct_recv, keep_send, keep_recv, fwd_send, fwd_recv,
    token_send, token_recv, total_send, total_recv, row_send, row_recv, state_send, state_recv, read_send, read_recv,
):
    n, t, s_count, members, group, heads, head, rows = sizes
    planes = n // members
    me, core = lax.axis_index("sp"), lax.axis_index("tp")
    plane, place = me // members, lax.rem(me, members)
    model = prompt.shape[2]
    part = model // t
    positions = prompt.shape[1]
    width = heads * head
    side = 2
    batches = 2 if heads % 2 == 0 else 1
    batch = heads // batches

    def class_of(p):
        return lax.rem(p, side) * (members // side) + p // side

    def member_of(q):
        return (q % (members // side)) * side + q // (members // side)

    def turn(a, z):
        return (1 + a + (2 * z) // planes) % 2

    def prompt_of(p, a):
        return class_of(p) + members * turn(a, plane)

    def columns(c):
        return pl.ds(pl.multiple_of(c * part, part), part)

    def peer(r):
        return partner(place, r, members)

    local = [
        pltpu.make_async_copy(prompt.at[prompt_of(place, 0)], blocks.at[0, place], local_sem.at[0]),
        pltpu.make_async_copy(prompt.at[prompt_of(place, 1)], blocks.at[1, place], local_sem.at[1]),
        pltpu.make_async_copy(w_forget, wf, local_sem.at[2]),
        pltpu.make_async_copy(w_value, wv, local_sem.at[3]),
        pltpu.make_async_copy(w_query, wq, local_sem.at[4]),
        pltpu.make_async_copy(w_outgate, wo, local_sem.at[5]),
    ]

    barrier = pltpu.get_barrier_semaphore()
    for o in range(1, n):
        pl.semaphore_signal(barrier, inc=1, device_id=(lax.rem(me + o, n), core), device_id_type=MESH)
    for o in range(1, t):
        pl.semaphore_signal(barrier, inc=1, device_id=(me, lax.rem(core + o, t)), device_id_type=MESH)
    for copy in local:
        copy.start()
    pl.semaphore_wait(barrier, n - 1 + t - 1)

    def direct(a, r):
        to = peer(r)
        return pltpu.make_async_remote_copy(
            src_ref=prompt.at[prompt_of(to, a), :, columns(core)],
            dst_ref=blocks.at[a, place, :, columns(core)],
            send_sem=direct_send.at[a, r], recv_sem=direct_recv.at[a, r],
            device_id=(plane * members + to, core), device_id_type=MESH,
        )

    def direct_in(a, r):
        frm = peer(r)
        return pltpu.make_async_remote_copy(
            src_ref=prompt.at[prompt_of(frm, a), :, columns(core)],
            dst_ref=blocks.at[a, frm, :, columns(core)],
            send_sem=direct_send.at[a, r], recv_sem=direct_recv.at[a, r],
            device_id=(plane * members + frm, core), device_id_type=MESH,
        )

    def keep_copy(r):
        return pltpu.make_async_remote_copy(
            src_ref=keep, dst_ref=keeps.at[r],
            send_sem=keep_send.at[r], recv_sem=keep_recv.at[r],
            device_id=(plane * members + peer(r), core), device_id_type=MESH,
        )

    def forward(a, r, o, c):
        piece = blocks.at[a, peer(r), :, columns(c)]
        return pltpu.make_async_remote_copy(
            src_ref=piece, dst_ref=piece,
            send_sem=fwd_send.at[a, r, o], recv_sem=fwd_recv.at[a, r, o],
            device_id=(me, lax.rem(core + o, t)), device_id_type=MESH,
        )

    def token_copy(o, c):
        return pltpu.make_async_remote_copy(
            src_ref=token, dst_ref=tokens.at[c],
            send_sem=token_send.at[o], recv_sem=token_recv.at[o],
            device_id=(me, lax.rem(core + o, t)), device_id_type=MESH,
        )

    for r in range(1, members):
        keep_copy(r).start()
    for a in range(2):
        for r in range(1, members):
            direct(a, r).start()
    for o in range(1, t):
        token_copy(o, core).start()

    keeps[0] = keep[...]
    tokens[core] = token[...]
    floor_row = floor[...]

    def value(a, r):
        p = peer(r)
        values[a, p] = jnp.dot(blocks[a, p], wv[...], preferred_element_type=F32).astype(BF16)

    def forget(a, r):
        p = peer(r)
        pre = jnp.dot(blocks[a, p], wf[...], preferred_element_type=F32)
        loss = floor_row * (1.0 / (1.0 + jnp.exp(pre)))
        row = keeps[r, pl.ds(prompt_of(place, a), 1), :]
        i0 = lax.broadcasted_iota(jnp.int32, (positions, positions), 0)
        i1 = lax.broadcasted_iota(jnp.int32, (positions, positions), 1)
        scale = jnp.sum(jnp.where(i0 == i1, jnp.broadcast_to(row, (positions, positions)), 0.0), axis=1, keepdims=True)
        log_forget = jnp.log(scale) + jnp.log1p(-loss)
        gate = 1.0 - scale + scale * loss
        later = jnp.where(i1 > i0, 1.0, 0.0).astype(BF16)
        inside = sum(jnp.dot(later, piece, preferred_element_type=F32) for piece in pieces(log_forget, 3))
        logs[a, pl.ds(p, 1), :] = inside[0:1] + log_forget[0:1]
        weighted[a, p] = gate * jnp.exp(inside)

    def total_copy(k, o, z):
        return pltpu.make_async_remote_copy(
            src_ref=totals.at[k, z], dst_ref=totals.at[k, z],
            send_sem=total_send.at[k, o], recv_sem=total_recv.at[k, o],
            device_id=(lax.rem(me + o * members, n), core), device_id_type=MESH,
        )

    def keeper(a, g):
        return prompt_of(place, a) * group + g

    def row_copy(a, g):
        return pltpu.make_async_remote_copy(
            src_ref=totals.at[turn(a, plane), plane], dst_ref=got_totals.at[plane],
            send_sem=row_send.at[a, g], recv_sem=row_recv.at[plane],
            device_id=(keeper(a, g), core), device_id_type=MESH,
        )

    def state_copy(a, g, b):
        return pltpu.make_async_remote_copy(
            src_ref=states.at[a, pl.ds(b * batch, batch), pl.ds(g * rows, rows), :],
            dst_ref=got_states.at[plane, pl.ds(b * batch, batch)],
            send_sem=state_send.at[a, g, b], recv_sem=state_recv.at[plane, b],
            device_id=(keeper(a, g), core), device_id_type=MESH,
        )

    def read_copy(o, sender):
        return pltpu.make_async_remote_copy(
            src_ref=reads.at[sender], dst_ref=reads.at[sender],
            send_sem=read_send.at[o], recv_sem=read_recv.at[o],
            device_id=(lax.rem(me + o, n), core), device_id_type=MESH,
        )

    def finish(a):
        suffixes, suffix = [None] * members, jnp.zeros((1, width), F32)
        for p in reversed(range(members)):
            suffixes[p] = suffix
            suffix = suffix + logs[a, p : p + 1, :]
        k = turn(a, plane)
        totals[k, plane] = suffix
        for o in range(1, planes):
            total_copy(k, o, plane).start()
        value(a, members - 1)
        for p in range(members):
            weighted[a, p] = weighted[a, p] * jnp.exp(suffixes[p])
        for h in range(heads):
            lanes = slice(h * head, (h + 1) * head)
            w = weighted[a, :, :, lanes].reshape(members * positions, head)
            v = values[a, :, :, lanes].reshape(members * positions, head)
            states[a, h] = sum(
                lax.dot_general(piece, v, (((0,), (0,)), ((), ())), preferred_element_type=F32)
                for piece in pieces(w, 2)
            )
        for g in range(group):

            @pl.when(keeper(a, g) != me)
            def _():
                row_copy(a, g).start()
                for b in range(batches if a == 0 else 1):
                    state_copy(a, g, b).start()

            @pl.when(keeper(a, g) == me)
            def _():
                got_totals[plane] = suffix
                got_states[plane] = states[a, :, g * rows : (g + 1) * rows, :]

    def send_reads():
        for o in range(1, planes):
            z = lax.rem(plane - o + planes, planes)
            for k in range(2):
                total_copy(k, o, z).wait_recv()
        for a in range(2):
            later = jnp.zeros((1, width), F32)
            for z in range(planes):
                later = later + jnp.where(z > plane, totals[turn(a, plane), z], 0.0)
            decay = jnp.exp(later)
            for h in range(heads):
                lanes = slice(h * head, (h + 1) * head)
                reads[me, a, :, lanes] = jnp.dot(
                    sums[3 + a, :, lanes] * decay[:, lanes], states[a, h],
                    preferred_element_type=F32, precision=lax.Precision.HIGHEST,
                )[0:1]
        for o in range(n - 1, 0, -1):
            read_copy(o, me).start()
        for g in range(group):

            @pl.when(keeper(1, g) != me)
            def _():
                for b in range(1, batches):
                    state_copy(1, g, b).start()

    for copy in local[:4]:
        copy.wait()

    def own_block(a, carry):
        forget(a, 0)
        value(a, 0)
        return carry

    lax.fori_loop(0, 2, own_block, 0)

    local[4].wait()
    local[5].wait()
    for o in range(1, t):
        token_copy(o, lax.rem(core - o + t, t)).wait_recv()
    feature = jnp.concatenate([tokens[c] for c in range(t)], axis=1)
    query = jnp.dot(feature, wq[...], preferred_element_type=F32)
    new_forget = jnp.dot(feature, wf[...], preferred_element_type=F32)
    new_value = jnp.dot(feature, wv[...], preferred_element_type=F32).astype(BF16).astype(F32)
    new_gate = jnp.dot(feature, wo[...], preferred_element_type=F32)
    new_loss = floor_row * (1.0 / (1.0 + jnp.exp(new_forget)))
    read_weight = query * (1.0 - new_loss)
    sums[0] = query * new_loss
    sums[1] = new_value
    sums[2] = new_gate * (1.0 / (1.0 + jnp.exp(-new_gate)))
    seq = lax.broadcasted_iota(jnp.int32, read_weight.shape, 0)
    for a in range(2):
        picked = jnp.where(seq == prompt_of(place, a), read_weight, 0.0)
        sums[3 + a] = jnp.broadcast_to(jnp.sum(picked, axis=0, keepdims=True), read_weight.shape)

    def arrive(a, r):
        direct_in(a, r).wait_recv()
        for o in range(1, t):
            forward(a, r, o, core).start()

    def ready(a, r):
        if a == 0:
            keep_copy(r).wait_recv()
        for o in range(1, t):
            forward(a, r, o, lax.rem(core - o + t, t)).wait_recv()

    arrive(0, 1)
    for a in range(2):

        def step(r, carry, a=a):
            arrive(a, r)
            ready(a, r - 1)
            forget(a, r - 1)
            value(a, r - 1)
            return carry

        lax.fori_loop(2, members, step, 0)
        if a == 0:
            arrive(1, 1)
        ready(a, members - 1)
        forget(a, members - 1)
        finish(a)
    send_reads()

    mine = me // group
    source = member_of(lax.rem(mine, members))
    for z in range(planes):

        @pl.when(z * members + source != me)
        def _():
            pairs = [(got_totals.at[z], row_recv.at[z])]
            for b in range(batches):
                pairs.append((got_states.at[z, pl.ds(b * batch, batch)], state_recv.at[z, b]))
            for piece, arrived in pairs:
                pltpu.make_async_remote_copy(
                    src_ref=piece, dst_ref=piece,
                    send_sem=row_send.at[0, 0], recv_sem=arrived,
                    device_id=(z * members + source, core), device_id_type=MESH,
                ).wait_recv()

    first = lax.rem(me, group) * rows
    i0 = lax.broadcasted_iota(jnp.int32, (rows, head), 0) + first
    i1 = lax.broadcasted_iota(jnp.int32, (rows, head), 1)
    later = jnp.zeros((1, width), F32)
    final = [got_states[planes - 1, h] for h in range(heads)]
    for z in reversed(range(planes - 1)):
        later = later + got_totals[z + 1]
        decay = jnp.exp(later)
        for h in range(heads):
            row = jnp.broadcast_to(decay[:, h * head : (h + 1) * head], (rows, head))
            final[h] = final[h] + got_states[z, h] * jnp.sum(jnp.where(i0 == i1, row, 0.0), axis=1, keepdims=True)
    for h in range(heads):
        cache_out[h] = final[h].astype(BF16)

    for o in range(1, n):
        read_copy(o, lax.rem(me - o + n, n)).wait_recv()
    for s in range(s_count):
        row = jnp.zeros((1, width), F32)
        for z in range(planes):
            a = (s // members + 1 + (2 * z) // planes) % 2
            row = row + reads[z * members + member_of(s % members), a]
        sums[5, s : s + 1, :] = row
    for h in range(heads):
        lanes = slice(h * head, (h + 1) * head)
        mixed = sums[5, :, lanes] + jnp.sum(sums[0, :, lanes], axis=1, keepdims=True) * sums[1, :, lanes]
        normed = mixed * lax.rsqrt(jnp.mean(mixed * mixed, axis=1, keepdims=True) + EPSILON)
        read_out[:, lanes] = (normed * gain[...] * sums[2, :, lanes]).astype(BF16)

    for r in range(1, members):
        keep_copy(r).wait_send()
    for o in range(1, t):
        token_copy(o, core).wait_send()
    for a in range(2):
        for r in range(1, members):
            direct(a, r).wait_send()
            for o in range(1, t):
                forward(a, r, o, core).wait_send()
        for o in range(1, planes):
            total_copy(a, o, plane).wait_send()
        for g in range(group):

            @pl.when(keeper(a, g) != me)
            def _():
                row_copy(a, g).wait_send()
                for b in range(batches):
                    state_copy(a, g, b).wait_send()

    for o in range(1, n):
        read_copy(o, me).wait_send()


def per_device(prompt, keep_scale, new_token, w_query, w_forget, w_value, w_outgate, floor_gap, norm_gain):
    n, t = lax.axis_size("sp"), lax.axis_size("tp")
    s_count, positions, model = prompt.shape
    head = norm_gain.shape[0]
    width = w_forget.shape[1]
    heads = width // head
    members = s_count // 2
    planes = n // members
    group = n // s_count
    rows = head // group
    batches = 2 if heads % 2 == 0 else 1
    sizes = (n, t, s_count, members, group, heads, head, rows)
    dma = pltpu.SemaphoreType.DMA
    vmem = pl.BlockSpec(memory_space=pltpu.VMEM)
    hbm = pl.BlockSpec(memory_space=pl.ANY)
    return pl.pallas_call(
        functools.partial(kernel, sizes),
        out_shape=(
            jax.ShapeDtypeStruct((heads, rows, head), BF16),
            jax.ShapeDtypeStruct((s_count, width), BF16),
        ),
        in_specs=[hbm, vmem, vmem, hbm, hbm, hbm, hbm, vmem, vmem],
        out_specs=(vmem, vmem),
        scratch_shapes=[
            pltpu.VMEM((2, members, positions, model), BF16),
            pltpu.VMEM((members,) + keep_scale.shape, F32),
            pltpu.VMEM((t,) + new_token.shape, BF16),
            pltpu.VMEM((model, width), BF16),
            pltpu.VMEM((model, width), BF16),
            pltpu.VMEM((model, width), BF16),
            pltpu.VMEM((model, width), BF16),
            pltpu.VMEM((2, members, positions, width), F32),
            pltpu.VMEM((2, members, positions, width), BF16),
            pltpu.VMEM((2, members, width), F32),
            pltpu.VMEM((2, planes, 1, width), F32),
            pltpu.VMEM((planes, 1, width), F32),
            pltpu.VMEM((2, heads, head, head), F32),
            pltpu.VMEM((planes, heads, rows, head), F32),
            pltpu.VMEM((n, 2, 1, width), F32),
            pltpu.VMEM((6, s_count, width), F32),
            dma((6,)),
            dma((2, members)), dma((2, members)),
            dma((members,)), dma((members,)),
            dma((2, members, t)), dma((2, members, t)),
            dma((t,)), dma((t,)),
            dma((2, planes)), dma((2, planes)),
            dma((2, group)), dma((planes,)),
            dma((2, group, batches)), dma((planes, batches)),
            dma((n,)), dma((n,)),
        ],
        compiler_params=pltpu.CompilerParams(collective_id=0, has_side_effects=True),
    )(
        prompt, keep_scale, new_token, w_query, w_forget, w_value, w_outgate,
        floor_gap.reshape(1, width), norm_gain.reshape(1, head),
    )


def solution(mesh):
    return jax.shard_map(
        per_device,
        mesh=mesh,
        in_specs=(
            P(None, "sp", None),
            P(None, "sp"),
            P(None, "tp"),
            P(None, "tp"),
            P(None, "tp"),
            P(None, "tp"),
            P(None, "tp"),
            P("tp"),
            P(),
        ),
        out_specs=(P("tp", "sp", None), P(None, "tp")),
        check_vma=False,
    )
```

time: 51.8 us -> 44.9 us (0.87)
  Pallas kernels: 48.1 us -> 41.2 us
    pallas_call x1, Pallas kernels: 48.1 us -> 41.2 us  [per_device(): pl.pallas_call(functools.partial(kernel, sizes), out_shape=(jax.ShapeDtyp...]
where the time goes in v2:
time: 44.9 us; the launch traced here: 44.6 us
  Pallas kernels  41.2 us (92%)
  local copies, waits for them, and re-layouts  2.77 us (6%)
  between operations  0.64 us (1%)
    pallas_call x1, Pallas kernels, per_device(): pl.pallas_call(functools.partial(kernel, sizes), out_shape=(jax.ShapeDtyp...  41.2 us
    unnamed x2, local copies, waits for them, and re-layouts  2.77 us

profile of v2, /device:TPU:0, one launch (start us, length us, event | category | flops | bytes accessed | tf_op | source)
XLA Modules:
  0.0 44.6 jit_solution(12949611180675967409)
XLA Ops:
  0.6 41.2 %shard_map.104 = (bf16[4,64,128]{2,1,0:T(8,128)(2,1)}, bf16[8,512]{1,0:T(8,128)(2,1)}) custom-call(bf16[8,64,2048]{2,1,0:T(8,128)(2,1)} %prompt.1, f32[8,64]{1,0:T(8,128)} %keep.1, bf16[8,1024]{1,0:T(8,128)(2,1)} %token_.1, bf16[2048,512]{1,0:T(8,128)(2,1)} %w_query.1, bf16[2048,512]{1,0:T(8,128)(2,1)} %w_forget.1, bf16[2048,512]{1,0:T(8,128)(2,1)} %w_value.1, ...), custom_call_target="tpu_custom_call" | custom-call | tf_op jit(solution)/shard_map/pallas_call | solution.py:390
  41.8 1.5 %copy.13 = bf16[4,64,128]{2,1,0:T(8,128)(2,1)} copy(bf16[4,64,128]{2,1,0:T(8,128)(2,1)} %get-tuple-element.4) | data formatting | bytes 131072
  43.3 1.3 %copy.14 = bf16[8,512]{1,0:T(8,128)(2,1)} copy(bf16[8,512]{1,0:T(8,128)(2,1)} %get-tuple-element.5) | data formatting | bytes 16384
